TPU v7x, 32 devices: a whole 2x2x4 slice. The times are simulated.
32 devices in a mesh: ep: 8 (over z, x), tp: 4 (over y, core).
Axes of the slice: x: 2, y: 2, z: 4, core: 2. Of those that a mesh axis runs over, the one named last changes fastest.
Arguments:
- query_rows: bfloat16 [2048, 1024], P('ep', 'tp'), may hold values from -8 to 8
- key_rows: bfloat16 [2048, 256], P('ep', 'tp'), may hold values from -8 to 8
- value_rows: bfloat16 [2048, 256], P('ep', 'tp'), may hold values from -16 to 16
- query_gain: float32 [64], replicated, may hold values from 0.5 to 7.5
- key_gain: float32 [64], replicated, may hold values from 0.5 to 7.5
- moe_tokens: bfloat16 [4096, 2048], P(('ep', 'tp')), may hold values from -6 to 6
- norm_gain: float32 [2048], replicated, may hold values from 0.1 to 1.9
- routes: int32 [4096, 2], P('ep'), may hold values from 0 to 7, all different within a row; in each aligned block of 128 rows (0 to 127, 128 to 255, ...) at most 64 rows name the same one
- route_weights: float32 [4096, 2], P('ep'), may hold values from 0.1 to 1
- expert_gate: bfloat16 [8, 2048, 1024], P('ep', None, 'tp'), may hold values from -0.125 to 0.125
- expert_up: bfloat16 [8, 2048, 1024], P('ep', None, 'tp'), may hold values from -0.125 to 0.125
- expert_down: bfloat16 [8, 1024, 2048], P('ep', 'tp'), may hold values from -0.1875 to 0.1875
- shared_gate: bfloat16 [2048, 1024], P(None, 'tp'), may hold values from -0.125 to 0.125
- shared_up: bfloat16 [2048, 1024], P(None, 'tp'), may hold values from -0.125 to 0.125
- shared_down: bfloat16 [1024, 2048], P('tp'), may hold values from -0.1875 to 0.1875
Outputs:
- attn_out: bfloat16 [2048, 1024], P('ep', 'tp')
- moe_out: bfloat16 [4096, 2048], P(('ep', 'tp'))
Inputs may be any that keep to these rules, and one draw needn't show every extreme that they name: `routes`: each row names 2 different experts. Within each aligned block of 128 rows no expert is named more than 64 times, and in every draw some expert is named exactly 64 times in some block.
All inputs are finite; a program needn't handle non-finite values.
Results may differ from a plain program's by a relative error of at most 0.012.
The roundings to bfloat16 on the way count: a program that leaves them out, or rounds other values in their place, can miss the bound.
Values may be sent and summed in bfloat16 or wider, within the bound.
A program may use at most 192 MiB of HBM per device.

v0:
```python
import jax
import jax.numpy as jnp
from jax import lax
from jax.sharding import PartitionSpec as P

GRID_W = 64
epsilon = 1e-06
rotary_base = 10000.0
routed_scale = 2.5


def rotate_heads(heads_in, gain_row, positions):
    values32 = heads_in.astype(jnp.float32)
    scaled = (
        values32
        * lax.rsqrt(jnp.mean(values32 * values32, axis=-1, keepdims=True) + epsilon)
        * gain_row
    )
    pair_count = scaled.shape[-1] // 4
    inv_freq = rotary_base ** (-jnp.arange(pair_count, dtype=jnp.float32) / pair_count)
    grid_row = (positions // GRID_W).astype(jnp.float32)
    grid_col = (positions % GRID_W).astype(jnp.float32)
    angles = jnp.concatenate([grid_row[:, None] * inv_freq, grid_col[:, None] * inv_freq], axis=-1)[
        :, None, :
    ]
    cosine = jnp.cos(angles)
    sine_part = jnp.sin(angles)
    first_half = scaled[..., 0::2]
    second_half = scaled[..., 1::2]
    turned = jnp.stack(
        [
            first_half * cosine - second_half * sine_part,
            first_half * sine_part + second_half * cosine,
        ],
        axis=-1,
    )
    return turned.reshape(scaled.shape).astype(jnp.bfloat16)


def span_length(row_count):
    length = min(row_count, 2048)
    while row_count % length:
        length -= 1
    return length


def attend(query_rows, key_rows, value_rows, query_gain, key_gain):
    row_count = query_rows.shape[0]
    head_size = query_gain.shape[0]
    q_heads = query_rows.shape[1] // head_size
    kv_heads = key_rows.shape[1] // head_size
    group = q_heads // kv_heads
    scale = head_size ** (-0.5)
    positions = lax.axis_index("ep") * row_count + jnp.arange(row_count, dtype=jnp.int32)
    q_rot = rotate_heads(query_rows.reshape(row_count, q_heads, head_size), query_gain, positions)
    k_rot = rotate_heads(key_rows.reshape(row_count, kv_heads, head_size), key_gain, positions)
    key_value = jnp.stack([k_rot, value_rows.reshape(row_count, kv_heads, head_size)], axis=2)
    key_value = key_value.reshape(row_count, kv_heads * 2 * head_size)
    q_grouped = q_rot.reshape(row_count, kv_heads, group, head_size).transpose(1, 2, 0, 3)
    q_grouped = q_grouped.reshape(kv_heads, group * row_count, head_size)
    query_count = group * row_count
    initial = (
        jnp.full((kv_heads, query_count), -jnp.inf, jnp.float32),
        jnp.zeros((kv_heads, query_count), jnp.float32),
        jnp.zeros((kv_heads, query_count, head_size), jnp.float32),
    )

    def one_span(carried, span_rows):
        run_max, run_sum, mixed = carried
        keys_span = span_rows[:, :, 0, :]
        values_span = span_rows[:, :, 1, :]
        scores = (
            jnp.einsum("hrd,shd->hrs", q_grouped, keys_span, preferred_element_type=jnp.float32)
            * scale
        )
        new_max = jnp.maximum(run_max, jnp.max(scores, axis=-1))
        factor = jnp.exp(run_max - new_max)
        weights = jnp.exp(scores - new_max[..., None])
        run_sum = run_sum * factor + jnp.sum(weights, axis=-1)
        added = jnp.einsum(
            "hrs,shd->hrd",
            weights.astype(jnp.bfloat16),
            values_span,
            preferred_element_type=jnp.float32,
        )
        mixed = mixed * factor[..., None] + added
        return ((new_max, run_sum, mixed), None)

    carried = initial
    piece_rows = lax.all_gather(key_value, "ep", axis=0, tiled=True)
    piece_count = piece_rows.shape[0]
    length = span_length(piece_count)
    spans = piece_rows.reshape(piece_count // length, length, kv_heads, 2, head_size)
    carried, unused = lax.scan(one_span, carried, spans)
    run_max, run_sum, mixed = carried
    result = (mixed / run_sum[..., None]).astype(jnp.bfloat16)
    result = result.reshape(kv_heads, group, row_count, head_size).transpose(2, 0, 1, 3)
    return result.reshape(row_count, q_heads * head_size)


def slot_ranks(route_rows, tok_rows, experts):
    top_count = route_rows.shape[1]
    blocks = route_rows.shape[0] // tok_rows
    chosen = route_rows.reshape(blocks, tok_rows * top_count)
    one_hot = (chosen[:, :, None] == jnp.arange(experts, dtype=jnp.int32)[None, None, :]).astype(
        jnp.int32
    )
    ranks = jnp.sum((jnp.cumsum(one_hot, axis=1) - one_hot) * one_hot, axis=2)
    return (chosen, ranks)


def build_send(source, chosen, ranks, tok_rows, top_count, capacity, experts):
    blocks = chosen.shape[0]
    model_width = source.shape[1]
    block_ids = jnp.arange(blocks, dtype=jnp.int32)[:, None]
    dest = (chosen * blocks + block_ids) * capacity + ranks
    rows_from = (
        block_ids * tok_rows
        + jnp.arange(tok_rows * top_count, dtype=jnp.int32)[None, :] // top_count
    )
    slot_rows = jnp.full((experts * blocks * capacity,), blocks * tok_rows, jnp.int32)
    slot_rows = slot_rows.at[dest.reshape(-1)].set(rows_from.reshape(-1))
    padded = jnp.concatenate([source, jnp.zeros((1, model_width), source.dtype)], axis=0)
    return padded[slot_rows].reshape(experts, blocks * capacity, model_width)


def expert_products(arrived, w_gate, w_up, w_down):
    gate_proj = jnp.einsum("lrd,ldf->lrf", arrived, w_gate, preferred_element_type=jnp.float32)
    up_proj = jnp.einsum("lrd,ldf->lrf", arrived, w_up, preferred_element_type=jnp.float32)
    hidden = (jax.nn.silu(gate_proj) * up_proj).astype(jnp.bfloat16)
    return jnp.einsum("lrf,lfd->lrd", hidden, w_down, preferred_element_type=jnp.float32)


def shared_products(rows_in, w_gate, w_up, w_down):
    gate_proj = jnp.dot(rows_in, w_gate, preferred_element_type=jnp.float32)
    up_proj = jnp.dot(rows_in, w_up, preferred_element_type=jnp.float32)
    hidden = (jax.nn.silu(gate_proj) * up_proj).astype(jnp.bfloat16)
    return jnp.dot(hidden, w_down, preferred_element_type=jnp.float32)


def experts_half(
    moe_tokens,
    norm_gain,
    routes,
    route_weights,
    expert_gate,
    expert_up,
    expert_down,
    shared_gate,
    shared_up,
    shared_down,
):
    tok_rows, model_width = moe_tokens.shape
    top_count = routes.shape[1]
    tp_size = lax.axis_size("tp")
    ep_size = lax.axis_size("ep")
    local_experts = expert_gate.shape[0]
    experts = local_experts * ep_size
    capacity = 2 * tok_rows * top_count // experts
    lane = lax.axis_index("tp")
    values32 = moe_tokens.astype(jnp.float32)
    normed = (
        values32
        * lax.rsqrt(jnp.mean(values32 * values32, axis=-1, keepdims=True) + epsilon)
        * norm_gain
    ).astype(jnp.bfloat16)
    gates = route_weights / jnp.sum(route_weights, axis=-1, keepdims=True) * routed_scale
    own_gates = lax.dynamic_slice_in_dim(gates, lane * tok_rows, tok_rows, 0)
    own_routes = lax.dynamic_slice_in_dim(routes, lane * tok_rows, tok_rows, 0)
    chosen, ranks = slot_ranks(own_routes, tok_rows, experts)
    send = build_send(normed, chosen, ranks, tok_rows, top_count, capacity, experts)
    landed = lax.all_to_all(send, "ep", split_axis=0, concat_axis=1, tiled=True)
    arrived, group_rows = (
        lax.all_gather(
            landed.reshape(local_experts, ep_size, 1, capacity, model_width),
            "tp",
            axis=2,
            tiled=True,
        ),
        lax.all_gather(normed.reshape(1, 1, 1, tok_rows, model_width), "tp", axis=2, tiled=True),
    )
    own_chosen = chosen[0]
    own_ranks = ranks[0]
    arrived = arrived.reshape(local_experts, ep_size * tp_size * capacity, model_width)
    routed_part = expert_products(arrived, expert_gate, expert_up, expert_down)
    shared_part = shared_products(
        group_rows.reshape(tp_size * tok_rows, model_width), shared_gate, shared_up, shared_down
    )
    routed_sum, shared_sum = (
        lax.psum_scatter(
            routed_part.reshape(local_experts, ep_size, tp_size, capacity, model_width).astype(
                jnp.bfloat16
            ),
            "tp",
            scatter_dimension=2,
            tiled=True,
        ).astype(jnp.float32),
        lax.psum_scatter(
            shared_part.reshape(1, 1, tp_size, tok_rows, model_width).astype(jnp.bfloat16),
            "tp",
            scatter_dimension=2,
            tiled=True,
        ).astype(jnp.float32),
    )
    outgoing = routed_sum.astype(jnp.bfloat16).reshape(
        local_experts, ep_size * capacity, model_width
    )
    returned = lax.all_to_all(outgoing, "ep", split_axis=1, concat_axis=0, tiled=True)
    flat_rows = returned.reshape(experts * capacity, model_width)
    picked = flat_rows[own_chosen * capacity + own_ranks].reshape(tok_rows, top_count, model_width)
    routed_total = jnp.sum(own_gates[:, :, None] * picked.astype(jnp.float32), axis=1)
    return (routed_total + shared_sum.reshape(tok_rows, model_width)).astype(jnp.bfloat16)


def body(
    query_rows,
    key_rows,
    value_rows,
    query_gain,
    key_gain,
    moe_tokens,
    norm_gain,
    routes,
    route_weights,
    expert_gate,
    expert_up,
    expert_down,
    shared_gate,
    shared_up,
    shared_down,
):
    attn_out = attend(query_rows, key_rows, value_rows, query_gain, key_gain)
    moe_out = experts_half(
        moe_tokens,
        norm_gain,
        routes,
        route_weights,
        expert_gate,
        expert_up,
        expert_down,
        shared_gate,
        shared_up,
        shared_down,
    )
    return (attn_out, moe_out)


def solution(mesh):
    return jax.shard_map(
        body,
        mesh=mesh,
        in_specs=(
            P("ep", "tp"),
            P("ep", "tp"),
            P("ep", "tp"),
            P(),
            P(),
            P(("ep", "tp"), None),
            P(),
            P("ep", None),
            P("ep", None),
            P("ep", None, "tp"),
            P("ep", None, "tp"),
            P("ep", "tp", None),
            P(None, "tp"),
            P(None, "tp"),
            P("tp", None),
        ),
        out_specs=(P("ep", "tp"), P(("ep", "tp"), None)),
        check_vma=False,
    )
```

profile of v0, /device:TPU:0, one launch (start us, length us, event | category | flops | bytes accessed | tf_op | source)
XLA Modules:
  0.0 441.3 jit_solution(13202950709804458420)
XLA Ops:
  13.5 3.3 gather_fusion
  16.8 55.6 %all_to_all.8 = bf16[8,64,2048]{2,1,0:T(8,128)(2,1)} all-to-all(bf16[8,64,2048]{2,1,0:T(8,128)(2,1)} %bitcast.110), channel_id=1, replica_groups=mesh['ep'=8,'tp'=4] {'ep'}, dimensions={0} | all-to-all | bytes 4194304 | tf_op jit(solution)/shard_map/all_to_all | solution.py:172
  73.3 56.7 %all-gather.5.cloned.1.call-done = bf16[8,256,2048]{2,1,0:T(8,128)(2,1)} async-done(((bf16[8,64,2048]{2,1,0:T(8,128)(2,1)}), bf16[8,256,2048]{2,1,0:T(8,128)(2,1)}) %all-gather.5.cloned.1.call-update) | async-done | bytes 8388624 | tf_op jit(solution)/shard_map/all_gather | solution.py:174
  129.9 5.9 %fusion.21 = f32[2048,256]{1,0:T(8,128)S(1)} fusion(bf16[2048,2048]{1,0:T(8,128)(2,1)} %bitcast.125, bf16[1,2048,256]{2,1,0:T(8,128)(2,1)S(1)} %copy-done.11), kind=kOutput, calls=%fused_computation.28 | convolution fusion | flops 2147483648 | bytes 11534336 | tf_op jit(solution)/shard_map/lrd,ldf->lrf/dot_general | solution.py:128
  135.9 2.6 fusion.4
  138.6 5.6 %convert_bitcast_fusion = bf16[1,8,4,64,2048]{4,3,2,1,0:T(8,128)(2,1)} fusion(bf16[8,4,64,256]{3,2,1,0:T(8,128)(2,1)S(1)} %bitcast.113, bf16[1,256,2048]{2,1,0:T(8,128)(2,1)S(1)} %copy-done), kind=kOutput, calls=%fused_computation.3 | convolution fusion | flops 2151677952 | bytes 10485760 | tf_op jit(solution)/shard_map/lrf,lfd->lrd/dot_general | solution.py:131
  146.3 8.4 %all-gather.7.cloned.1.call-done = bf16[512,2048]{1,0:T(8,128)(2,1)} async-done(((bf16[128,2048]{1,0:T(8,128)(2,1)}), bf16[512,2048]{1,0:T(8,128)(2,1)}) %all-gather.7.cloned.1.call-update) | async-done | bytes 2097168 | tf_op jit(solution)/shard_map/all_gather | solution.py:180
  154.6 3.5 fusion.56
  158.2 5.4 %convolution_convert_fusion = bf16[512,2048]{1,0:T(8,128)(2,1)} fusion(bf16[256,2048]{1,0:T(8,128)(2,1)} %param.29, bf16[512,2048]{1,0:T(8,128)(2,1)S(1)} %copy-done.10, bf16[2048,256]{1,0:T(8,128)(2,1)} %param.28, f32[512,256]{1,0:T(8,128)} %fusion.56), kind=kOutput, calls=%fused_computation.9 | convolution fusion | flops 1075576832 | bytes 6815744 | tf_op jit(solution)/shard_map/dot_general | solution.py:138
  163.5 146.5 %all-reduce.4.cloned.1.call-done = bf16[1,8,4,64,2048]{4,3,2,1,0:T(8,128)(2,1)} async-done(((bf16[1,8,4,64,2048]{4,3,2,1,0:T(8,128)(2,1)}), bf16[1,8,4,64,2048]{4,3,2,1,0:T(8,128)(2,1)}) %all-reduce.4.cloned.1.call-update) | async-done | bytes 8388624
  310.0 2.5 constant_dynamic-slice_fusion
  312.5 5.2 %copy.56 = bf16[1,512,2048]{2,0,1:T(2,128)(2,1)} copy(bf16[1,512,2048]{2,1,0:T(8,128)(2,1)S(1)} %bitcast.111) | data formatting | bytes 4194304 | tf_op jit(solution)/shard_map/reshape | solution.py:205
  318.2 13.2 %reduce.9 = bf16[512,2048]{1,0:T(8,128)(2,1)S(1)} reduce(bf16[512,1,2048]{2,1,0:T(2,128)(2,1)} %bitcast.108, bf16[]{:T(256)} %broadcast.377), dimensions={1}, to_apply=%bitcast.106.reduce_sub_computation | reduce | bytes 4194306
  331.4 3.8 reshape.653
  335.2 5.6 %all-to-all-start.1 = ((bf16[8,2,65536]{2,1,0:T(2,128)(2,1)}), bf16[8,2,65536]{2,1,0:T(2,128)(2,1)S(1)}, u32[]{:S(2)}, u32[]{:S(2)}) async-start(bf16[8,2,65536]{2,1,0:T(2,128)(2,1)} %reshape.653), calls=%async_computation.1 | async-start | bytes 4194304 | tf_op jit(solution)/shard_map/all_to_all | solution.py:208
  341.7 68.2 %all_gather.9 = bf16[2048,128]{0,1:T(8,128)(2,1)S(1)} all-gather(bf16[256,128]{0,1:T(8,128)(2,1)S(1)} %bitcast.119), channel_id=1, replica_groups=mesh['ep'=8,'tp'=4] {'ep'}, dimensions={0}, use_global_device_ids=true | all-gather | bytes 589824 | tf_op jit(solution)/shard_map/all_gather | solution.py:90
  411.3 1.9 fusion
  413.2 1.7 fusion.12
  415.8 4.4 reshape.654
  420.2 3.5 copy.55
  423.7 2.3 gather_fusion.1
  426.0 2.5 reshape.614
  428.5 4.1 multiply_reduce_fusion.1
  432.5 2.3 fusion.18
  (94 shorter events, 12.6 us)
Async XLA Ops:
  7.2 131.4 %copy-start = (bf16[1,256,2048]{2,1,0:T(8,128)(2,1)S(1)}, bf16[1,256,2048]{2,1,0:T(8,128)(2,1)}, u32[]{:S(2)}) copy-start(bf16[1,256,2048]{2,1,0:T(8,128)(2,1)} %param.26) | copy-start | bytes 3145732
  7.2 122.7 %all-gather.5.cloned.1.call-start = ((), (), s32[]{:S(2)}) async-start(), calls=%async_computation.4 | async-start | bytes 10485760 | tf_op jit(solution)/shard_map/all_gather | solution.py:174
  13.4 3.4 copy-start.2
  72.4 57.5 %copy-start.11 = (bf16[1,2048,256]{2,1,0:T(8,128)(2,1)S(1)}, bf16[1,2048,256]{2,1,0:T(8,128)(2,1)}, u32[]{:S(2)}) copy-start(bf16[1,2048,256]{2,1,0:T(8,128)(2,1)} %param.24) | copy-start | bytes 3145732
  72.5 82.2 %all-gather.7.cloned.1.call-start = ((), (), s32[]{:S(2)}) async-start(), calls=%async_computation.5 | async-start | bytes 2621440 | tf_op jit(solution)/shard_map/all_gather | solution.py:180
  73.2 236.8 %all-reduce.4.cloned.1.call-start = ((), (), s32[]{:S(2)}) async-start(), calls=%async_computation.6 | async-start | bytes 16777216
  129.9 5.9 %copy-start.9 = (bf16[8,256,2048]{2,1,0:T(8,128)(2,1)S(1)}, bf16[8,256,2048]{2,1,0:T(8,128)(2,1)}, u32[]{:S(2)}) copy-start(bf16[8,256,2048]{2,1,0:T(8,128)(2,1)} %all-gather.5.cloned.1.call-done) | copy-start | bytes 25165828
  129.9 6.0 %copy-start.12 = (bf16[1,2048,256]{2,1,0:T(8,128)(2,1)S(1)}, bf16[1,2048,256]{2,1,0:T(8,128)(2,1)}, u32[]{:S(2)}) copy-start(bf16[1,2048,256]{2,1,0:T(8,128)(2,1)} %param.25) | copy-start | bytes 3145732
  144.1 0.9 copy-start.4
  144.1 1.1 copy-start.7
  144.1 1.3 copy-start.3
  144.1 1.3 copy-start.8
  144.1 1.4 copy-start.6
  144.1 1.5 copy-start.13
  144.2 288.4 %reduce-scatter.5.cloned.1.call-start = ((), (), s32[]{:S(2)}) async-start(), calls=%async_computation.3 | async-start | bytes 2621440 | tf_op jit(solution)/shard_map/reduce_scatter | solution.py:198
  154.6 3.5 copy-start.10
  335.2 6.4 %copy-start.5 = (bf16[256,64]{0,1:T(8,128)(2,1)S(1)}, bf16[256,64]{0,1:T(8,128)(2,1)}, u32[]{:S(2)}) copy-start(bf16[256,64]{0,1:T(8,128)(2,1)} %param.17) | copy-start | bytes 98308
  335.2 80.5 %all-to-all-start.1 = ((bf16[8,2,65536]{2,1,0:T(2,128)(2,1)}), bf16[8,2,65536]{2,1,0:T(2,128)(2,1)S(1)}, u32[]{:S(2)}, u32[]{:S(2)}) async-start(bf16[8,2,65536]{2,1,0:T(2,128)(2,1)} %reshape.653), calls=%async_computation.1 | async-start | bytes 4194304 | tf_op jit(solution)/shard_map/all_to_all | solution.py:208
  426.0 8.8 %copy-start.1 = (bf16[1,256,2048]{2,1,0:T(8,128)(2,1)S(1)}, bf16[1,256,2048]{2,1,0:T(8,128)(2,1)}, u32[]{:S(2)}) copy-start(bf16[1,256,2048]{2,1,0:T(8,128)(2,1)} %param.26) | copy-start | bytes 3145732
Sparse Core Ops, SparseCore 0:
  72.6 57.2 all-gather.4
  132.0 22.5 all-gather.6
  157.1 152.8 all-reduce.3
  312.4 31.3 reduce-scatter.4
where the time goes:
time: 442 us; the launch traced here: 441 us
  waiting for transfers between devices  212 us (48%)
  blocking collectives  124 us (28%)
  local copies, waits for them, and re-layouts  33 us (7%)
  other arithmetic  26.2 us (6%)
  matrix products  26 us (6%)
  between operations  14.2 us (3%)
  starting transfers between devices  5.97 us (1%)
    unnamed x5, waiting for transfers between devices  147 us
    all_gather x1, blocking collectives, attend(): piece_rows = lax.all_gather(key_value, 'ep', axis=0, tiled=True)  68.2 us
    all_gather x1, waiting for transfers between devices, experts_half(): lax.all_gather(landed.reshape(local_experts, ep_size, 1, capacity, model_...  56.7 us
    all_to_all x1, blocking collectives, experts_half(): landed = lax.all_to_all(send, 'ep', split_axis=0, concat_axis=1, tiled=True)  55.6 us
    unnamed x37, local copies, waits for them, and re-layouts  16.9 us
    unnamed x1, other arithmetic  13.2 us
  transfers between devices with their start and end apart: 5, of which 3 were waited for; matrix products, arithmetic and copies ran while one was open for 16% of the time, Pallas kernels for 0%

commit v1 on v0

--- a/solution.py
+++ b/solution.py
@@ -87,7 +87,22 @@
         return ((new_max, run_sum, mixed), None)
 
     carried = initial
-    piece_rows = lax.all_gather(key_value, "ep", axis=0, tiled=True)
+
+    def serve_the_desk(x0):
+        shares = lax.axis_size("ep")
+        all_blocks = list(map(lambda to_i: (to_i, (to_i + 1) % shares), range(shares)))
+
+        def _try_all_panel(arr_next):
+            if len(arr_next) == shares:
+                return arr_next
+            built = _try_all_panel([lax.ppermute(arr_next[0], "ep", all_blocks), *arr_next])
+            return built
+
+        found_now = jnp.concatenate(_try_all_panel([x0]), axis=0)
+        w_next = jnp.roll(found_now, (lax.axis_index("ep") + 1) * x0.shape[0], axis=0)
+        return w_next
+
+    piece_rows = serve_the_desk(key_value)
     piece_count = piece_rows.shape[0]
     length = span_length(piece_count)
     spans = piece_rows.reshape(piece_count // length, length, kv_heads, 2, head_size)

time: 442 us -> 415 us (0.939)
  blocking collectives: 124 us -> 55.6 us
  waiting for transfers between devices: 212 us -> 240 us
  local copies, waits for them, and re-layouts: 33 us -> 44.3 us
    all_gather x1 -> x0, blocking collectives: 68.2 us -> none  [attend(): piece_rows = lax.all_gather(key_value, 'ep', axis=0, tiled=True)]
    ppermute x0 -> x7, waiting for transfers between devices: none -> 46 us  [_try_all_panel(): lax.ppermute(arr_next[0], 'ep', all_blocks)]
    unnamed x5, waiting for transfers between devices: 147 us -> 106 us
    all_to_all x1, waiting for transfers between devices: 0.01 us -> 31.2 us  [experts_half(): lax.all_to_all(outgoing, 'ep', split_axis=1, concat_axis=0, tiled=True)]
    unnamed x37 -> x52, local copies, waits for them, and re-layouts: 16.9 us -> 26.5 us
    all_gather x1, waiting for transfers between devices: 8.37 us -> 0.01 us  [experts_half(): lax.all_gather(normed.reshape(1, 1, 1, tok_rows, model_width), 'tp', axis...]
  transfers between devices with their start and end apart: 5 -> 12, of which waited for: 3 -> 10; matrix products, arithmetic and copies ran while one was open for 16% -> 20% of each run, Pallas kernels for 0% -> 0%
where the time goes in v1:
time: 415 us; the launch traced here: 414 us
  waiting for transfers between devices  240 us (58%)
  blocking collectives  55.6 us (13%)
  local copies, waits for them, and re-layouts  44.3 us (11%)
  matrix products  26.6 us (6%)
  other arithmetic  26.2 us (6%)
  between operations  14.2 us (3%)
  starting transfers between devices  7.19 us (2%)
    unnamed x5, waiting for transfers between devices  106 us
    all_gather x1, waiting for transfers between devices, experts_half(): lax.all_gather(landed.reshape(local_experts, ep_size, 1, capacity, model_...  56.7 us
    all_to_all x1, blocking collectives, experts_half(): landed = lax.all_to_all(send, 'ep', split_axis=0, concat_axis=1, tiled=True)  55.6 us
    ppermute x7, waiting for transfers between devices, _try_all_panel(): lax.ppermute(arr_next[0], 'ep', all_blocks)  46 us
    all_to_all x1, waiting for transfers between devices, experts_half(): lax.all_to_all(outgoing, 'ep', split_axis=1, concat_axis=0, tiled=True)  31.2 us
    unnamed x52, local copies, waits for them, and re-layouts  26.5 us
    unnamed x1, other arithmetic  13.2 us
  transfers between devices with their start and end apart: 12, of which 10 were waited for; matrix products, arithmetic and copies ran while one was open for 20% of the time, Pallas kernels for 0%

profile of v1, /device:TPU:0, one launch (start us, length us, event | category | flops | bytes accessed | tf_op | source)
XLA Modules:
  0.0 414.1 jit_solution(17729098434502324406)
XLA Ops:
  13.5 3.3 gather_fusion
  16.8 55.6 %all_to_all.8 = bf16[8,64,2048]{2,1,0:T(8,128)(2,1)} all-to-all(bf16[8,64,2048]{2,1,0:T(8,128)(2,1)} %bitcast.110), channel_id=1, replica_groups=mesh['ep'=8,'tp'=4] {'ep'}, dimensions={0} | all-to-all | bytes 4194304 | tf_op jit(solution)/shard_map/all_to_all | solution.py:187
  73.3 56.7 %all-gather.5.cloned.1.call-done = bf16[8,256,2048]{2,1,0:T(8,128)(2,1)} async-done(((bf16[8,64,2048]{2,1,0:T(8,128)(2,1)}), bf16[8,256,2048]{2,1,0:T(8,128)(2,1)}) %all-gather.5.cloned.1.call-update) | async-done | bytes 8388624 | tf_op jit(solution)/shard_map/all_gather | solution.py:189
  129.9 6.0 %fusion.21 = f32[2048,256]{1,0:T(8,128)S(1)} fusion(bf16[2048,2048]{1,0:T(8,128)(2,1)} %bitcast.127, bf16[1,2048,256]{2,1,0:T(8,128)(2,1)S(1)} %copy-done.11), kind=kOutput, calls=%fused_computation.28 | convolution fusion | flops 2147483648 | bytes 11534336 | tf_op jit(solution)/shard_map/lrd,ldf->lrf/dot_general | solution.py:143
  136.0 2.8 fusion.4
  138.7 5.6 %convert_bitcast_fusion = bf16[1,8,4,64,2048]{4,3,2,1,0:T(8,128)(2,1)} fusion(bf16[8,4,64,256]{3,2,1,0:T(8,128)(2,1)S(1)} %bitcast.113, bf16[1,256,2048]{2,1,0:T(8,128)(2,1)S(1)} %copy-done), kind=kOutput, calls=%fused_computation.3 | convolution fusion | flops 2151677952 | bytes 10485760 | tf_op jit(solution)/shard_map/lrf,lfd->lrd/dot_general | solution.py:146
  147.3 5.3 %collective-permute-done = bf16[256,128]{0,1:T(8,128)(2,1)S(1)} collective-permute-done((bf16[256,128]{0,1:T(8,128)(2,1)S(1)}, bf16[256,128]{0,1:T(8,128)(2,1)S(1)}, u32[]{:S(2)}, u32[]{:S(2)}) %collective-permute-start) | collective-permute-done | bytes 65568 | tf_op jit(solution)/shard_map/ppermute | solution.py:98
  152.8 6.8 %collective-permute-done.1 = bf16[256,128]{0,1:T(8,128)(2,1)S(1)} collective-permute-done((bf16[256,128]{0,1:T(8,128)(2,1)S(1)}, bf16[256,128]{0,1:T(8,128)(2,1)S(1)}, u32[]{:S(2)}, u32[]{:S(2)}) %collective-permute-start.1) | collective-permute-done | bytes 65568 | tf_op jit(solution)/shard_map/ppermute | solution.py:98
  159.7 6.8 %collective-permute-done.2 = bf16[256,128]{0,1:T(8,128)(2,1)S(1)} collective-permute-done((bf16[256,128]{0,1:T(8,128)(2,1)S(1)}, bf16[256,128]{0,1:T(8,128)(2,1)S(1)}, u32[]{:S(2)}, u32[]{:S(2)}) %collective-permute-start.2) | collective-permute-done | bytes 65568 | tf_op jit(solution)/shard_map/ppermute | solution.py:98
  166.7 6.8 %collective-permute-done.3 = bf16[256,128]{0,1:T(8,128)(2,1)S(1)} collective-permute-done((bf16[256,128]{0,1:T(8,128)(2,1)S(1)}, bf16[256,128]{0,1:T(8,128)(2,1)S(1)}, u32[]{:S(2)}, u32[]{:S(2)}) %collective-permute-start.3) | collective-permute-done | bytes 65568 | tf_op jit(solution)/shard_map/ppermute | solution.py:98
  173.5 7.1 %collective-permute-done.4 = bf16[256,128]{0,1:T(8,128)(2,1)S(1)} collective-permute-done((bf16[256,128]{0,1:T(8,128)(2,1)S(1)}, bf16[256,128]{0,1:T(8,128)(2,1)S(1)}, u32[]{:S(2)}, u32[]{:S(2)}) %collective-permute-start.4) | collective-permute-done | bytes 65568 | tf_op jit(solution)/shard_map/ppermute | solution.py:98
  181.5 6.1 %collective-permute-done.5 = bf16[256,128]{0,1:T(8,128)(2,1)S(1)} collective-permute-done((bf16[256,128]{0,1:T(8,128)(2,1)S(1)}, bf16[256,128]{0,1:T(8,128)(2,1)S(1)}, u32[]{:S(2)}, u32[]{:S(2)}) %collective-permute-start.5) | collective-permute-done | bytes 65568 | tf_op jit(solution)/shard_map/ppermute | solution.py:98
  187.7 7.0 %collective-permute-done.6 = bf16[256,128]{0,1:T(8,128)(2,1)S(1)} collective-permute-done((bf16[256,128]{0,1:T(8,128)(2,1)S(1)}, bf16[256,128]{0,1:T(8,128)(2,1)S(1)}, u32[]{:S(2)}, u32[]{:S(2)}) %collective-permute-start.6) | collective-permute-done | bytes 65568 | tf_op jit(solution)/shard_map/ppermute | solution.py:98
  195.3 3.6 fusion.56
  198.9 5.7 %convolution_convert_fusion = bf16[512,2048]{1,0:T(8,128)(2,1)} fusion(bf16[256,2048]{1,0:T(8,128)(2,1)} %param.29, bf16[512,2048]{1,0:T(8,128)(2,1)S(1)} %copy-done.10, bf16[2048,256]{1,0:T(8,128)(2,1)} %param.28, f32[512,256]{1,0:T(8,128)} %fusion.56), kind=kOutput, calls=%fused_computation.9 | convolution fusion | flops 1075576832 | bytes 6815744 | tf_op jit(solution)/shard_map/dot_general | solution.py:153
  204.6 105.4 %all-reduce.4.cloned.1.call-done = bf16[1,8,4,64,2048]{4,3,2,1,0:T(8,128)(2,1)} async-done(((bf16[1,8,4,64,2048]{4,3,2,1,0:T(8,128)(2,1)}), bf16[1,8,4,64,2048]{4,3,2,1,0:T(8,128)(2,1)}) %all-reduce.4.cloned.1.call-update) | async-done | bytes 8388624
  312.5 5.2 %copy.56 = bf16[1,512,2048]{2,0,1:T(2,128)(2,1)} copy(bf16[1,512,2048]{2,1,0:T(8,128)(2,1)S(1)} %bitcast.111) | data formatting | bytes 4194304 | tf_op jit(solution)/shard_map/reshape | solution.py:220
  318.2 13.2 %reduce.9 = bf16[512,2048]{1,0:T(8,128)(2,1)S(1)} reduce(bf16[512,1,2048]{2,1,0:T(2,128)(2,1)} %bitcast.108, bf16[]{:T(256)} %broadcast.383), dimensions={1}, to_apply=%bitcast.106.reduce_sub_computation | reduce | bytes 4194306
  331.4 3.8 reshape.653
  335.2 5.5 %all-to-all-start.1 = ((bf16[8,2,65536]{2,1,0:T(2,128)(2,1)}), bf16[8,2,65536]{2,1,0:T(2,128)(2,1)S(1)}, u32[]{:S(2)}, u32[]{:S(2)}) async-start(bf16[8,2,65536]{2,1,0:T(2,128)(2,1)} %reshape.653), calls=%async_computation.1 | async-start | bytes 4194304 | tf_op jit(solution)/shard_map/all_to_all | solution.py:223
  357.4 31.2 %all-to-all-done.1 = bf16[8,2,65536]{2,1,0:T(2,128)(2,1)S(1)} async-done(((bf16[8,2,65536]{2,1,0:T(2,128)(2,1)}), bf16[8,2,65536]{2,1,0:T(2,128)(2,1)S(1)}, u32[]{:S(2)}, u32[]{:S(2)}) %all-to-all-start.1) | async-done | bytes 2097184 | tf_op jit(solution)/shard_map/all_to_all | solution.py:223
  388.6 4.4 %reshape.654 = bf16[512,1,2048]{2,1,0:T(2,128)(2,1)} reshape(bf16[8,2,65536]{2,1,0:T(2,128)(2,1)S(1)} %all-to-all-done.1) | data formatting | bytes 4194304
  393.0 3.5 copy.55
  401.3 4.1 multiply_reduce_fusion.1
  (124 shorter events, 38.5 us)
Async XLA Ops:
  7.2 131.6 %copy-start = (bf16[1,256,2048]{2,1,0:T(8,128)(2,1)S(1)}, bf16[1,256,2048]{2,1,0:T(8,128)(2,1)}, u32[]{:S(2)}) copy-start(bf16[1,256,2048]{2,1,0:T(8,128)(2,1)} %param.26) | copy-start | bytes 3145732
  7.2 122.7 %all-gather.5.cloned.1.call-start = ((), (), s32[]{:S(2)}) async-start(), calls=%async_computation.4 | async-start | bytes 10485760 | tf_op jit(solution)/shard_map/all_gather | solution.py:189
  13.4 3.4 copy-start.2
  72.4 57.5 %copy-start.11 = (bf16[1,2048,256]{2,1,0:T(8,128)(2,1)S(1)}, bf16[1,2048,256]{2,1,0:T(8,128)(2,1)}, u32[]{:S(2)}) copy-start(bf16[1,2048,256]{2,1,0:T(8,128)(2,1)} %param.24) | copy-start | bytes 3145732
  72.5 122.8 %all-gather.7.cloned.1.call-start = ((), (), s32[]{:S(2)}) async-start(), calls=%async_computation.5 | async-start | bytes 2621440 | tf_op jit(solution)/shard_map/all_gather | solution.py:195
  73.2 236.8 %all-reduce.4.cloned.1.call-start = ((), (), s32[]{:S(2)}) async-start(), calls=%async_computation.6 | async-start | bytes 16777216
  129.9 6.0 %copy-start.9 = (bf16[8,256,2048]{2,1,0:T(8,128)(2,1)S(1)}, bf16[8,256,2048]{2,1,0:T(8,128)(2,1)}, u32[]{:S(2)}) copy-start(bf16[8,256,2048]{2,1,0:T(8,128)(2,1)} %all-gather.5.cloned.1.call-done) | copy-start | bytes 25165828
  129.9 6.0 %copy-start.12 = (bf16[1,2048,256]{2,1,0:T(8,128)(2,1)S(1)}, bf16[1,2048,256]{2,1,0:T(8,128)(2,1)}, u32[]{:S(2)}) copy-start(bf16[1,2048,256]{2,1,0:T(8,128)(2,1)} %param.25) | copy-start | bytes 3145732
  144.3 1.3 copy-start.5
  144.3 2.8 copy-start.4
  144.3 8.3 %copy-start.8 = (f32[64]{0:T(128)S(1)}, f32[64]{0:T(128)}, u32[]{:S(2)}) copy-start(f32[64]{0:T(128)} %param.18) | copy-start | bytes 772
  144.3 22.2 %copy-start.6 = (f32[512,2]{0,1:T(2,128)S(1)}, f32[512,2]{0,1:T(2,128)}, u32[]{:S(2)}) copy-start(f32[512,2]{0,1:T(2,128)} %param.23) | copy-start | bytes 12292
  144.3 36.6 %copy-start.13 = (u32[32]{0:T(128)S(1)}, u32[32]{0:T(128)}, u32[]{:S(2)}) copy-start(u32[32]{0:T(128)} %constant.148) | copy-start | bytes 388
  144.4 261.0 %reduce-scatter.5.cloned.1.call-start = ((), (), s32[]{:S(2)}) async-start(), calls=%async_computation.3 | async-start | bytes 2621440 | tf_op jit(solution)/shard_map/reduce_scatter | solution.py:213
  145.6 7.0 %collective-permute-start = (bf16[256,128]{0,1:T(8,128)(2,1)S(1)}, bf16[256,128]{0,1:T(8,128)(2,1)S(1)}, u32[]{:S(2)}, u32[]{:S(2)}) collective-permute-start(bf16[256,128]{0,1:T(8,128)(2,1)S(1)} %bitcast.117), channel_id=1, source_target_pairs={{0,4},{4,8},{8,12},{12,16},{16,20},{20,24},{24,28},{28,0},{1,5},{5... | collective-permute-start | bytes 196616 | tf_op jit(solution)/shard_map/ppermute | solution.py:98
  152.6 7.0 %collective-permute-start.1 = (bf16[256,128]{0,1:T(8,128)(2,1)S(1)}, bf16[256,128]{0,1:T(8,128)(2,1)S(1)}, u32[]{:S(2)}, u32[]{:S(2)}) collective-permute-start(bf16[256,128]{0,1:T(8,128)(2,1)S(1)} %collective-permute-done), channel_id=1, source_target_pairs={{0,4},{4,8},{8,12},{12,16},{16,20},{20,24},{24,28},{28,0},{1,5},{5... | collective-permute-start | bytes 196616 | tf_op jit(solution)/shard_map/ppermute | solution.py:98
  159.6 7.0 %collective-permute-start.2 = (bf16[256,128]{0,1:T(8,128)(2,1)S(1)}, bf16[256,128]{0,1:T(8,128)(2,1)S(1)}, u32[]{:S(2)}, u32[]{:S(2)}) collective-permute-start(bf16[256,128]{0,1:T(8,128)(2,1)S(1)} %collective-permute-done.1), channel_id=1, source_target_pairs={{0,4},{4,8},{8,12},{12,16},{16,20},{20,24},{24,28},{28,0},{1,5},{5... | collective-permute-start | bytes 196616 | tf_op jit(solution)/shard_map/ppermute | solution.py:98
  166.5 7.0 %collective-permute-start.3 = (bf16[256,128]{0,1:T(8,128)(2,1)S(1)}, bf16[256,128]{0,1:T(8,128)(2,1)S(1)}, u32[]{:S(2)}, u32[]{:S(2)}) collective-permute-start(bf16[256,128]{0,1:T(8,128)(2,1)S(1)} %collective-permute-done.2), channel_id=1, source_target_pairs={{0,4},{4,8},{8,12},{12,16},{16,20},{20,24},{24,28},{28,0},{1,5},{5... | collective-permute-start | bytes 196616 | tf_op jit(solution)/shard_map/ppermute | solution.py:98
  173.5 7.2 %collective-permute-start.4 = (bf16[256,128]{0,1:T(8,128)(2,1)S(1)}, bf16[256,128]{0,1:T(8,128)(2,1)S(1)}, u32[]{:S(2)}, u32[]{:S(2)}) collective-permute-start(bf16[256,128]{0,1:T(8,128)(2,1)S(1)} %collective-permute-done.3), channel_id=1, source_target_pairs={{0,4},{4,8},{8,12},{12,16},{16,20},{20,24},{24,28},{28,0},{1,5},{5... | collective-permute-start | bytes 196616 | tf_op jit(solution)/shard_map/ppermute | solution.py:98
  180.6 7.0 %collective-permute-start.5 = (bf16[256,128]{0,1:T(8,128)(2,1)S(1)}, bf16[256,128]{0,1:T(8,128)(2,1)S(1)}, u32[]{:S(2)}, u32[]{:S(2)}) collective-permute-start(bf16[256,128]{0,1:T(8,128)(2,1)S(1)} %collective-permute-done.4), channel_id=1, source_target_pairs={{0,4},{4,8},{8,12},{12,16},{16,20},{20,24},{24,28},{28,0},{1,5},{5... | collective-permute-start | bytes 196616 | tf_op jit(solution)/shard_map/ppermute | solution.py:98
  187.7 7.0 %collective-permute-start.6 = (bf16[256,128]{0,1:T(8,128)(2,1)S(1)}, bf16[256,128]{0,1:T(8,128)(2,1)S(1)}, u32[]{:S(2)}, u32[]{:S(2)}) collective-permute-start(bf16[256,128]{0,1:T(8,128)(2,1)S(1)} %collective-permute-done.5), channel_id=1, source_target_pairs={{0,4},{4,8},{8,12},{12,16},{16,20},{20,24},{24,28},{28,0},{1,5},{5... | collective-permute-start | bytes 196616 | tf_op jit(solution)/shard_map/ppermute | solution.py:98
  195.3 3.6 copy-start.10
  335.2 53.4 %all-to-all-start.1 = ((bf16[8,2,65536]{2,1,0:T(2,128)(2,1)}), bf16[8,2,65536]{2,1,0:T(2,128)(2,1)S(1)}, u32[]{:S(2)}, u32[]{:S(2)}) async-start(bf16[8,2,65536]{2,1,0:T(2,128)(2,1)} %reshape.653), calls=%async_computation.1 | async-start | bytes 4194304 | tf_op jit(solution)/shard_map/all_to_all | solution.py:223
  398.8 8.8 %copy-start.1 = (bf16[1,256,2048]{2,1,0:T(8,128)(2,1)S(1)}, bf16[1,256,2048]{2,1,0:T(8,128)(2,1)}, u32[]{:S(2)}) copy-start(bf16[1,256,2048]{2,1,0:T(8,128)(2,1)} %param.26) | copy-start | bytes 3145732
  (2 other events, 1.6 us)
Sparse Core Ops, SparseCore 0:
  72.6 57.2 all-gather.4
  132.0 22.5 all-gather.6
  157.1 152.8 all-reduce.3
  312.4 31.3 reduce-scatter.4
